TPU v7x, 512 devices: a whole 4x4x16 slice. The times are simulated.
512 devices in a mesh: kv: 16 (over y, x), tp: 32 (over z, core).
Axes of the slice: x: 4, y: 4, z: 16, core: 2. Of those that a mesh axis runs over, the one named last changes fastest.
Arguments:
- residual: bfloat16 [512, 2048], P('tp', 'kv'), may hold values from -64 to 64
- prior_state: float32 [512, 16, 128, 128], P('tp', 'kv'), may hold values from -6 to 6
- w_query: bfloat16 [2048, 2048], P('tp', 'kv'), may hold values from -0.125 to 0.125
- w_forget: bfloat16 [2048, 2048], P('tp', 'kv'), may hold values from -0.125 to 0.125
- w_value: bfloat16 [2048, 2048], P('tp', 'kv'), may hold values from -0.125 to 0.125
- w_outgate: bfloat16 [2048, 2048], P('tp', 'kv'), may hold values from -0.125 to 0.125
- forget_floor: float32 [2048], P('kv'), may hold values from 0.05 to 0.9
- group_gain: float32 [2048], P('kv'), may hold values from 0.1 to 1.9
- w_mix_out: bfloat16 [2048, 2048], P('kv', 'tp'), may hold values from -0.397747564 to 0.397747564
- gain_mix_pre: float32 [2048], replicated, may hold values from 0.1 to 1.9
- gain_mix_post: float32 [2048], replicated, may hold values from 0.05 to 1.9
- gain_mlp_pre: float32 [2048], replicated, may hold values from 0.1 to 1.9
- gain_mlp_post: float32 [2048], replicated, may hold values from 0.1 to 1.9
- w_up: bfloat16 [2048, 8192], P('tp', 'kv'), may hold values from -0.125 to 0.125
- w_down: bfloat16 [8192, 2048], P('kv', 'tp'), may hold values from -0.198873782 to 0.198873782
Outputs:
- layer_out: bfloat16 [512, 2048], P('tp', 'kv')
- new_state: float32 [512, 16, 128, 128], P('tp', 'kv')
All inputs are finite; a program needn't handle non-finite values.
Results may differ from a plain program's by a relative error of at most 0.015.
Values may be sent and summed in bfloat16 or wider, within the bound.
No kernel may reach another device: no remote copies, remote signals or barrier semaphores. Data moves between devices by JAX's collectives and lax.ppermute only.
A program may use at most 64 MiB of HBM per device.

v0:
```python
import jax
import jax.numpy as jnp
from jax import lax
from jax.sharding import Mesh
from jax.sharding import PartitionSpec as P

HEAD_DIM = 128
KV = ("y", "x")
TP = ("z", "c")
epsilon = 1e-06


def inverse_norm(values):
    return lax.rsqrt(jnp.mean(values * values, axis=-1, keepdims=True) + epsilon)


def exchange(blocks, axes):
    return lax.all_to_all(blocks, axes, 0, 0, tiled=True)


def from_everyone(value, axes):
    devices = lax.axis_size(axes)
    return exchange(jnp.broadcast_to(value[None], (devices, *value.shape)), axes)


def shards(
    residual,
    prior_state,
    w_query,
    w_forget,
    w_value,
    w_outgate,
    forget_floor,
    group_gain,
    w_mix_out,
    gain_mix_pre,
    gain_mix_post,
    gain_mlp_pre,
    gain_mlp_post,
    w_up,
    w_down,
):
    batch_rows, own_cols = residual.shape
    groups = lax.axis_size(KV)
    full_width = groups * own_cols
    place = lax.axis_index(KV)
    head_cols = w_query.shape[1]
    hidden = w_up.shape[1]
    own_weights = jnp.concatenate(
        (w_query, w_forget, w_value, w_outgate, w_mix_out.T, w_up, w_down.T), axis=1
    )
    weights = lax.all_gather(own_weights, TP, axis=0, tiled=True)
    at = 4 * head_cols
    w_in = weights[:, :at]
    w_mix = weights[:, at : at + w_mix_out.shape[0]]
    at += w_mix_out.shape[0]
    w_up_all = weights[:, at : at + hidden]
    w_down_all = weights[:, at + hidden :]
    stream = from_everyone(residual, KV).astype(jnp.float32)
    scale = lax.rsqrt(jnp.sum(stream * stream, axis=(0, 2), keepdims=True) / full_width + epsilon)
    normed = (stream * scale * gain_mix_pre.reshape(groups, 1, own_cols)).astype(jnp.bfloat16)
    normed = normed.transpose(1, 0, 2).reshape(batch_rows, full_width)
    pre = jnp.dot(normed, w_in, preferred_element_type=jnp.float32).astype(jnp.bfloat16)
    query_pre, forget_pre, value_pre, gate_pre = (
        p.astype(jnp.float32) for p in jnp.split(pre, 4, axis=1)
    )
    query = jax.nn.silu(query_pre)
    forget = forget_floor + (1.0 - forget_floor) * jax.nn.sigmoid(forget_pre)
    new_state = (
        forget[:, :, None] * prior_state[:, 0] + (1.0 - forget)[:, :, None] * value_pre[:, None, :]
    )
    readout = jnp.einsum("bk,bkv->bv", query, new_state, precision=lax.Precision.HIGHEST)
    gated = (readout * inverse_norm(readout) * group_gain * jax.nn.sigmoid(gate_pre)).astype(
        jnp.bfloat16
    )
    mixed_part = lax.dot_general(
        gated, w_mix, (((1,), (1,)), ((), ())), preferred_element_type=jnp.float32
    )
    mixed = exchange(mixed_part.astype(jnp.bfloat16).reshape(batch_rows, groups, own_cols), KV)
    mixed = jnp.sum(mixed.astype(jnp.float32), axis=0)
    mix_scale = lax.rsqrt(jnp.sum(mixed * mixed) / full_width + epsilon)
    own_row = lax.dynamic_index_in_dim(stream, place, 1, keepdims=False)
    after_row = (own_row + mixed * mix_scale * gain_mix_post.reshape(groups, own_cols)).astype(
        jnp.bfloat16
    )
    after = from_everyone(after_row, KV).astype(jnp.float32)
    after_scale = lax.rsqrt(
        jnp.sum(after * after, axis=(1, 2), keepdims=True) / full_width + epsilon
    )
    hidden_in = (after * after_scale * gain_mlp_pre.reshape(groups, own_cols)).astype(jnp.bfloat16)
    up_sum = jnp.dot(
        hidden_in.reshape(batch_rows, full_width), w_up_all, preferred_element_type=jnp.float32
    )
    squared = jnp.square(jax.nn.relu(up_sum)).astype(jnp.bfloat16)
    channel_part = lax.dot_general(
        squared, w_down_all, (((1,), (1,)), ((), ())), preferred_element_type=jnp.float32
    )
    channel = exchange(
        channel_part.astype(jnp.bfloat16).reshape(batch_rows, groups, own_cols).transpose(1, 0, 2),
        KV,
    )
    channel = jnp.sum(channel.astype(jnp.float32), axis=0)
    out_gain = lax.dynamic_index_in_dim(
        gain_mlp_post.reshape(groups, own_cols), place, 0, keepdims=True
    )
    after_own = lax.dynamic_index_in_dim(after, place, 1, keepdims=False)
    layer_out = (after_own + channel * out_gain).astype(jnp.bfloat16)
    return (layer_out, new_state[:, None])


def solution(mesh):
    grid = Mesh(mesh.devices.reshape(4, 4, 16, 2), (*KV, *TP))
    return jax.shard_map(
        shards,
        mesh=grid,
        in_specs=(
            P(TP, KV),
            P(TP, KV, None, None),
            P(TP, KV),
            P(TP, KV),
            P(TP, KV),
            P(TP, KV),
            P(KV),
            P(KV),
            P(KV, TP),
            P(),
            P(),
            P(),
            P(),
            P(TP, KV),
            P(KV, TP),
        ),
        out_specs=(P(TP, KV), P(TP, KV, None, None)),
        check_vma=False,
    )
```

profile of v0, /device:TPU:32, one launch (start us, length us, event | category | flops | bytes accessed | tf_op | source)
XLA Modules:
  0.0 153.1 jit_solution(12552396937788839422)
XLA Ops:
  7.2 0.7 constant_dynamic-update-slice_fusion.5
  8.0 0.7 constant_dynamic-update-slice_fusion.4
  8.7 0.7 constant_dynamic-update-slice_fusion.3
  9.4 0.7 constant_dynamic-update-slice_fusion.2
  10.1 0.7 constant_dynamic-update-slice_fusion.1
  10.9 0.8 constant_dynamic-update-slice_fusion
  11.7 0.8 bitcast_dynamic-update-slice_fusion
  12.6 0.7 copy-done.1
  13.3 1.3 broadcast_in_dim.4
  14.6 7.0 %all-to-all-start = ((bf16[16,16,128]{2,1,0:T(8,128)(2,1)}), bf16[16,16,128]{2,1,0:T(8,128)(2,1)S(1)}, u32[]{:S(2)}, u32[]{:S(2)}) async-start(bf16[16,16,128]{2,1,0:T(8,128)(2,1)} %broadcast_in_dim.4), calls=%async_computation | async-start | bytes 131072 | tf_op jit(solution)/shard_map/all_to_all | solution.py:18
  22.3 7.0 %all-to-all-done = bf16[16,16,128]{2,1,0:T(8,128)(2,1)S(1)} async-done(((bf16[16,16,128]{2,1,0:T(8,128)(2,1)}), bf16[16,16,128]{2,1,0:T(8,128)(2,1)S(1)}, u32[]{:S(2)}, u32[]{:S(2)}) %all-to-all-start) | async-done | bytes 65568 | tf_op jit(solution)/shard_map/all_to_all | solution.py:18
  29.4 65.2 %all-gather.2.cloned.1.call-done = bf16[2048,1664]{1,0:T(8,128)(2,1)} async-done(((bf16[64,1664]{1,0:T(8,128)(2,1)}), bf16[2048,1664]{1,0:T(8,128)(2,1)}) %all-gather.2.cloned.1.call-update) | async-done | bytes 6815760 | tf_op jit(solution)/shard_map/all_gather | solution.py:52
  94.7 2.0 %fusion.20 = bf16[16,512]{1,0:T(8,128)(2,1)S(1)} fusion(bf16[2048,1664]{1,0:T(8,128)(2,1)} %all-gather.2.cloned.1.call-done, f32[16,128]{1,0:T(8,128)} %bitcast.60, f32[16]{0:T(128)S(1)} %add_rsqrt_fusion.2, bf16[16,16,128]{2,1,0:T(8,128)(2,1)S(1)} %all-to-all-done), kind=kOutput, calls=%fused_computation.12 | convolution fusion | flops 33693696 | bytes 2187328 | tf_op jit(solution)/shard_map/dot_general | solution.py:63
  97.4 2.6 %fusion.24 = f32[16,1,128]{2,1,0:T(1,128)S(1)} fusion(f32[16,128,1]{1,2,0:T(1,128)S(1)} %bitcast.56, f32[16,1,128,128]{3,2,1,0:T(8,128)} %param.16, f32[16,128]{1,0:T(8,128)S(1)} %slice_convert_fusion, f32[16,128]{1,0:T(8,128)S(1)} %get-tuple-element.3, f32[16,128]{1,0:T(8,128)S(1)} %get-tuple-element.2), kind=kOutput, calls=%fused_computation.15 | convolution fusion | flops 3932160 | bytes 1089536 | tf_op jit(solution)/shard_map/bk,bkv->bv/dot_general | solution.py:72
  100.1 1.3 fusion.8
  102.1 6.8 %all-to-all-start.1 = ((bf16[16,16,128]{2,1,0:T(8,128)(2,1)}), bf16[16,16,128]{2,1,0:T(8,128)(2,1)S(1)}, u32[]{:S(2)}, u32[]{:S(2)}) async-start(bf16[16,16,128]{2,1,0:T(8,128)(2,1)} %bitcast.22), calls=%async_computation.1 | async-start | bytes 131072 | tf_op jit(solution)/shard_map/all_to_all | solution.py:18
  109.0 7.6 %all-to-all-done.1 = bf16[16,16,128]{2,1,0:T(8,128)(2,1)S(1)} async-done(((bf16[16,16,128]{2,1,0:T(8,128)(2,1)}), bf16[16,16,128]{2,1,0:T(8,128)(2,1)S(1)}, u32[]{:S(2)}, u32[]{:S(2)}) %all-to-all-start.1) | async-done | bytes 65568 | tf_op jit(solution)/shard_map/all_to_all | solution.py:18
  117.9 0.7 fusion.43
  119.3 3.5 %all-to-all-start.2 = ((bf16[16,16,128]{2,1,0:T(8,128)(2,1)}), bf16[16,16,128]{2,1,0:T(8,128)(2,1)S(1)}, u32[]{:S(2)}, u32[]{:S(2)}) async-start(bf16[16,16,128]{2,1,0:T(8,128)(2,1)} %broadcast_in_dim.5), calls=%async_computation.2 | async-start | bytes 131072 | tf_op jit(solution)/shard_map/all_to_all | solution.py:18
  122.8 2.8 %multiply_add_fusion = f32[16,1,128,128]{3,2,1,0:T(8,128)} fusion(f32[16,1,128,128]{3,2,1,0:T(8,128)} %param.16, f32[16,128]{1,0:T(8,128)S(1)} %slice_convert_fusion, f32[16,128]{1,0:T(8,128)S(1)} %get-tuple-element.3, f32[16,128]{1,0:T(8,128)S(1)} %get-tuple-element.2), kind=kLoop, calls=%fused_computation.16 | loop fusion | flops 786432 | bytes 2121728 | tf_op jit(solution)/shard_map/add | solution.py:70
  125.6 4.8 %all-to-all-done.2 = bf16[16,16,128]{2,1,0:T(8,128)(2,1)S(1)} async-done(((bf16[16,16,128]{2,1,0:T(8,128)(2,1)}), bf16[16,16,128]{2,1,0:T(8,128)(2,1)S(1)}, u32[]{:S(2)}, u32[]{:S(2)}) %all-to-all-start.2) | async-done | bytes 65568 | tf_op jit(solution)/shard_map/all_to_all | solution.py:18
  130.7 3.2 %fusion.5 = bf16[2,16,8,128]{3,2,1,0:T(8,128)(2,1)S(1)} fusion(bf16[2048,1664]{1,0:T(8,128)(2,1)} %all-gather.2.cloned.1.call-done, bf16[2,8,16,128]{3,2,1,0:T(8,128)(2,1)S(1)} %bitcast.53), kind=kOutput, calls=%fused_computation.7 | convolution fusion | flops 67166208 | bytes 4325376 | tf_op jit(solution)/shard_map/dot_general | solution.py:95
  134.6 3.5 %all-to-all-start.3 = ((bf16[16,16,128]{2,1,0:T(8,128)(2,1)}), bf16[16,16,128]{2,1,0:T(8,128)(2,1)S(1)}, u32[]{:S(2)}, u32[]{:S(2)}) async-start(bf16[16,16,128]{2,1,0:T(8,128)(2,1)} %bitcast.51), calls=%async_computation.3 | async-start | bytes 131072 | tf_op jit(solution)/shard_map/all_to_all | solution.py:18
  138.1 7.6 %all-to-all-done.3 = bf16[16,16,128]{2,1,0:T(8,128)(2,1)S(1)} async-done(((bf16[16,16,128]{2,1,0:T(8,128)(2,1)}), bf16[16,16,128]{2,1,0:T(8,128)(2,1)S(1)}, u32[]{:S(2)}, u32[]{:S(2)}) %all-to-all-start.3) | async-done | bytes 65568 | tf_op jit(solution)/shard_map/all_to_all | solution.py:18
  (29 shorter events, 5.2 us)
Async XLA Ops:
  7.2 15.1 %copy-start = (f32[2048]{0:T(1024)S(1)}, f32[2048]{0:T(1024)}, u32[]{:S(2)}) copy-start(f32[2048]{0:T(1024)} %param.27) | copy-start | bytes 24580
  7.2 123.4 %copy-start.2 = (f32[2048]{0:T(1024)S(1)}, f32[2048]{0:T(1024)}, u32[]{:S(2)}) copy-start(f32[2048]{0:T(1024)} %param.26) | copy-start | bytes 24580
  7.2 87.5 %all-gather.2.cloned.1.call-start = ((), (), s32[]{:S(2)}) async-start(), calls=%async_computation.4 | async-start | bytes 7028736 | tf_op jit(solution)/shard_map/all_gather | solution.py:52
  12.6 0.7 copy-start.1
  14.6 14.7 %all-to-all-start = ((bf16[16,16,128]{2,1,0:T(8,128)(2,1)}), bf16[16,16,128]{2,1,0:T(8,128)(2,1)S(1)}, u32[]{:S(2)}, u32[]{:S(2)}) async-start(bf16[16,16,128]{2,1,0:T(8,128)(2,1)} %broadcast_in_dim.4), calls=%async_computation | async-start | bytes 131072 | tf_op jit(solution)/shard_map/all_to_all | solution.py:18
  102.1 14.5 %all-to-all-start.1 = ((bf16[16,16,128]{2,1,0:T(8,128)(2,1)}), bf16[16,16,128]{2,1,0:T(8,128)(2,1)S(1)}, u32[]{:S(2)}, u32[]{:S(2)}) async-start(bf16[16,16,128]{2,1,0:T(8,128)(2,1)} %bitcast.22), calls=%async_computation.1 | async-start | bytes 131072 | tf_op jit(solution)/shard_map/all_to_all | solution.py:18
  119.3 11.1 %all-to-all-start.2 = ((bf16[16,16,128]{2,1,0:T(8,128)(2,1)}), bf16[16,16,128]{2,1,0:T(8,128)(2,1)S(1)}, u32[]{:S(2)}, u32[]{:S(2)}) async-start(bf16[16,16,128]{2,1,0:T(8,128)(2,1)} %broadcast_in_dim.5), calls=%async_computation.2 | async-start | bytes 131072 | tf_op jit(solution)/shard_map/all_to_all | solution.py:18
  134.6 11.1 %all-to-all-start.3 = ((bf16[16,16,128]{2,1,0:T(8,128)(2,1)}), bf16[16,16,128]{2,1,0:T(8,128)(2,1)S(1)}, u32[]{:S(2)}, u32[]{:S(2)}) async-start(bf16[16,16,128]{2,1,0:T(8,128)(2,1)} %bitcast.51), calls=%async_computation.3 | async-start | bytes 131072 | tf_op jit(solution)/shard_map/all_to_all | solution.py:18
Sparse Core Ops, SparseCore 0:
  13.4 81.2 all-gather.1
where the time goes:
time: 154 us; the launch traced here: 153 us
  waiting for transfers between devices  92.2 us (60%)
  starting transfers between devices  20.9 us (14%)
  between operations  14.8 us (10%)
  local copies, waits for them, and re-layouts  9.3 us (6%)
  matrix products  9.19 us (6%)
  other arithmetic  6.68 us (4%)
    all_gather x1, waiting for transfers between devices, shards(): weights = lax.all_gather(own_weights, TP, axis=0, tiled=True)  65.2 us
    all_to_all x4, waiting for transfers between devices, exchange(): return lax.all_to_all(blocks, axes, 0, 0, tiled=True)  27 us
    all_to_all x4, starting transfers between devices, exchange(): return lax.all_to_all(blocks, axes, 0, 0, tiled=True)  20.8 us
    unnamed x13, local copies, waits for them, and re-layouts  5.83 us
    dot_general x1, matrix products, shards(): lax.dot_general(squared, w_down_all, (((1,), (1,)), ((), ())), preferred_...  3.21 us
  transfers between devices with their start and end apart: 5, of which 5 were waited for; matrix products, arithmetic and copies ran while one was open for 3% of the time, Pallas kernels for 0%

commit v1 on v0

--- a/solution.py
+++ b/solution.py
@@ -49,7 +49,9 @@
     own_weights = jnp.concatenate(
         (w_query, w_forget, w_value, w_outgate, w_mix_out.T, w_up, w_down.T), axis=1
     )
-    weights = lax.all_gather(own_weights, TP, axis=0, tiled=True)
+    weights = jnp.concatenate(
+        lax.all_to_all(jnp.stack([own_weights] * lax.axis_size(TP)), TP, 0, 0), axis=0
+    )
     at = 4 * head_cols
     w_in = weights[:, :at]
     w_mix = weights[:, at : at + w_mix_out.shape[0]]

time: 154 us -> 386 us (2.51)
  waiting for transfers between devices: 92.2 us -> 325 us
  starting transfers between devices: 20.9 us -> 34.4 us
  between operations: 14.8 us -> 1.54 us
    all_to_all x0 -> x1, waiting for transfers between devices: none -> 302 us  [shards(): lax.all_to_all(jnp.stack([own_weights] * lax.axis_size(TP)), TP, 0, 0)]
    all_gather x1 -> x0, waiting for transfers between devices: 65.2 us -> none  [shards(): weights = lax.all_gather(own_weights, TP, axis=0, tiled=True)]
    all_to_all x0 -> x1, starting transfers between devices: none -> 15.5 us  [shards(): lax.all_to_all(jnp.stack([own_weights] * lax.axis_size(TP)), TP, 0, 0)]
  transfers between devices with their start and end apart: 5 -> 5, of which waited for: 5 -> 5; matrix products, arithmetic and copies ran while one was open for 3% -> 2% of each run, Pallas kernels for 0% -> 0%
where the time goes in v1:
time: 386 us; the launch traced here: 385 us
  waiting for transfers between devices  325 us (84%)
  starting transfers between devices  34.4 us (9%)
  local copies, waits for them, and re-layouts  12.4 us (3%)
  matrix products  7.92 us (2%)
    all_to_all x1, waiting for transfers between devices, shards(): lax.all_to_all(jnp.stack([own_weights] * lax.axis_size(TP)), TP, 0, 0)  302 us
    all_to_all x4, waiting for transfers between devices, exchange(): return lax.all_to_all(blocks, axes, 0, 0, tiled=True)  23.6 us
    all_to_all x4, starting transfers between devices, exchange(): return lax.all_to_all(blocks, axes, 0, 0, tiled=True)  18.9 us
    all_to_all x1, starting transfers between devices, shards(): lax.all_to_all(jnp.stack([own_weights] * lax.axis_size(TP)), TP, 0, 0)  15.5 us
  transfers between devices with their start and end apart: 5, of which 5 were waited for; matrix products, arithmetic and copies ran while one was open for 2% of the time, Pallas kernels for 0%

profile of v1, /device:TPU:32, one launch (start us, length us, event | category | flops | bytes accessed | tf_op | source)
XLA Modules:
  0.0 384.9 jit_solution(10323041970228822793)
XLA Ops:
  0.6 1.3 broadcast_in_dim.4
  2.0 7.0 %all-to-all-start = ((bf16[16,16,128]{2,1,0:T(8,128)(2,1)}), bf16[16,16,128]{2,1,0:T(8,128)(2,1)S(1)}, u32[]{:S(2)}, u32[]{:S(2)}) async-start(bf16[16,16,128]{2,1,0:T(8,128)(2,1)} %broadcast_in_dim.4), calls=%async_computation | async-start | bytes 131072 | tf_op jit(solution)/shard_map/all_to_all | solution.py:18
  9.0 0.7 constant_dynamic-update-slice_fusion.5
  9.7 0.7 constant_dynamic-update-slice_fusion.4
  10.5 0.7 constant_dynamic-update-slice_fusion.3
  11.2 0.7 constant_dynamic-update-slice_fusion.2
  11.9 0.7 constant_dynamic-update-slice_fusion.1
  12.6 0.8 constant_dynamic-update-slice_fusion
  13.5 0.8 bitcast_dynamic-update-slice_fusion
  14.3 2.3 all-to-all-done
  16.7 3.7 stack.2
  20.4 15.5 %all-to-all-start.1 = ((bf16[32,64,1664]{2,1,0:T(8,128)(2,1)}), bf16[32,64,1664]{2,1,0:T(8,128)(2,1)}, u32[]{:S(2)}, u32[]{:S(2)}) async-start(bf16[32,64,1664]{2,1,0:T(8,128)(2,1)} %stack.2), calls=%async_computation.1 | async-start | bytes 13631488 | tf_op jit(solution)/shard_map/all_to_all | solution.py:53
  36.2 301.7 %all-to-all-done.1 = bf16[32,64,1664]{2,1,0:T(8,128)(2,1)} async-done(((bf16[32,64,1664]{2,1,0:T(8,128)(2,1)}), bf16[32,64,1664]{2,1,0:T(8,128)(2,1)}, u32[]{:S(2)}, u32[]{:S(2)}) %all-to-all-start.1) | async-done | bytes 6815776 | tf_op jit(solution)/shard_map/all_to_all | solution.py:53
  337.9 2.0 fusion.20
  339.9 1.4 fusion.24
  341.5 1.3 fusion.8
  343.4 4.9 %all-to-all-start.2 = ((bf16[16,16,128]{2,1,0:T(8,128)(2,1)}), bf16[16,16,128]{2,1,0:T(8,128)(2,1)S(1)}, u32[]{:S(2)}, u32[]{:S(2)}) async-start(bf16[16,16,128]{2,1,0:T(8,128)(2,1)} %bitcast.23), calls=%async_computation.2 | async-start | bytes 131072 | tf_op jit(solution)/shard_map/all_to_all | solution.py:18
  348.3 7.6 %all-to-all-done.2 = bf16[16,16,128]{2,1,0:T(8,128)(2,1)S(1)} async-done(((bf16[16,16,128]{2,1,0:T(8,128)(2,1)}), bf16[16,16,128]{2,1,0:T(8,128)(2,1)S(1)}, u32[]{:S(2)}, u32[]{:S(2)}) %all-to-all-start.2) | async-done | bytes 65568 | tf_op jit(solution)/shard_map/all_to_all | solution.py:18
  358.0 3.5 all-to-all-start.3
  361.5 1.6 multiply_add_fusion
  363.0 6.0 %all-to-all-done.3 = bf16[16,16,128]{2,1,0:T(8,128)(2,1)S(1)} async-done(((bf16[16,16,128]{2,1,0:T(8,128)(2,1)}), bf16[16,16,128]{2,1,0:T(8,128)(2,1)S(1)}, u32[]{:S(2)}, u32[]{:S(2)}) %all-to-all-start.3) | async-done | bytes 65568 | tf_op jit(solution)/shard_map/all_to_all | solution.py:18
  369.4 3.2 fusion.5
  373.2 3.5 all-to-all-start.4
  376.8 7.6 %all-to-all-done.4 = bf16[16,16,128]{2,1,0:T(8,128)(2,1)S(1)} async-done(((bf16[16,16,128]{2,1,0:T(8,128)(2,1)}), bf16[16,16,128]{2,1,0:T(8,128)(2,1)S(1)}, u32[]{:S(2)}, u32[]{:S(2)}) %all-to-all-start.4) | async-done | bytes 65568 | tf_op jit(solution)/shard_map/all_to_all | solution.py:18
  (37 shorter events, 3.9 us)
Async XLA Ops:
  0.6 35.3 %copy-start = (f32[2048]{0:T(1024)S(1)}, f32[2048]{0:T(1024)}, u32[]{:S(2)}) copy-start(f32[2048]{0:T(1024)} %param.27) | copy-start | bytes 24580
  2.0 14.7 %all-to-all-start = ((bf16[16,16,128]{2,1,0:T(8,128)(2,1)}), bf16[16,16,128]{2,1,0:T(8,128)(2,1)S(1)}, u32[]{:S(2)}, u32[]{:S(2)}) async-start(bf16[16,16,128]{2,1,0:T(8,128)(2,1)} %broadcast_in_dim.4), calls=%async_computation | async-start | bytes 131072 | tf_op jit(solution)/shard_map/all_to_all | solution.py:18
  20.4 15.6 %copy-start.4 = (f32[128]{0:T(128)S(1)}, f32[128]{0:T(128)}, u32[]{:S(2)}) copy-start(f32[128]{0:T(128)} %param.21) | copy-start | bytes 1540
  20.4 317.5 %copy-start.6 = (f32[2048]{0:T(1024)S(1)}, f32[2048]{0:T(1024)}, u32[]{:S(2)}) copy-start(f32[2048]{0:T(1024)} %param.24) | copy-start | bytes 24580
  20.4 319.5 %copy-start.1 = (f32[16,1,128,128]{3,2,1,0:T(8,128)S(1)}, f32[16,1,128,128]{3,2,1,0:T(8,128)}, u32[]{:S(2)}) copy-start(f32[16,1,128,128]{3,2,1,0:T(8,128)} %param.16) | copy-start | bytes 3145732
  20.4 321.1 %copy-start.5 = (f32[128]{0:T(128)S(1)}, f32[128]{0:T(128)}, u32[]{:S(2)}) copy-start(f32[128]{0:T(128)} %param.22) | copy-start | bytes 1540
  20.4 336.9 %copy-start.2 = (f32[2048]{0:T(1024)S(1)}, f32[2048]{0:T(1024)}, u32[]{:S(2)}) copy-start(f32[2048]{0:T(1024)} %param.25) | copy-start | bytes 24580
  20.4 317.5 %all-to-all-start.1 = ((bf16[32,64,1664]{2,1,0:T(8,128)(2,1)}), bf16[32,64,1664]{2,1,0:T(8,128)(2,1)}, u32[]{:S(2)}, u32[]{:S(2)}) async-start(bf16[32,64,1664]{2,1,0:T(8,128)(2,1)} %stack.2), calls=%async_computation.1 | async-start | bytes 13631488 | tf_op jit(solution)/shard_map/all_to_all | solution.py:53
  35.9 333.3 %copy-start.3 = (f32[2048]{0:T(1024)S(1)}, f32[2048]{0:T(1024)}, u32[]{:S(2)}) copy-start(f32[2048]{0:T(1024)} %param.26) | copy-start | bytes 24580
  343.4 12.5 %all-to-all-start.2 = ((bf16[16,16,128]{2,1,0:T(8,128)(2,1)}), bf16[16,16,128]{2,1,0:T(8,128)(2,1)S(1)}, u32[]{:S(2)}, u32[]{:S(2)}) async-start(bf16[16,16,128]{2,1,0:T(8,128)(2,1)} %bitcast.23), calls=%async_computation.2 | async-start | bytes 131072 | tf_op jit(solution)/shard_map/all_to_all | solution.py:18
  358.0 11.1 %all-to-all-start.3 = ((bf16[16,16,128]{2,1,0:T(8,128)(2,1)}), bf16[16,16,128]{2,1,0:T(8,128)(2,1)S(1)}, u32[]{:S(2)}, u32[]{:S(2)}) async-start(bf16[16,16,128]{2,1,0:T(8,128)(2,1)} %broadcast_in_dim.5), calls=%async_computation.3 | async-start | bytes 131072 | tf_op jit(solution)/shard_map/all_to_all | solution.py:18
  373.2 11.1 %all-to-all-start.4 = ((bf16[16,16,128]{2,1,0:T(8,128)(2,1)}), bf16[16,16,128]{2,1,0:T(8,128)(2,1)S(1)}, u32[]{:S(2)}, u32[]{:S(2)}) async-start(bf16[16,16,128]{2,1,0:T(8,128)(2,1)} %bitcast.52), calls=%async_computation.4 | async-start | bytes 131072 | tf_op jit(solution)/shard_map/all_to_all | solution.py:18
